TPU v7x, 32 devices: a whole 2x2x4 slice. The times are simulated.
32 devices in a mesh: grp: 2 (over y), sp: 4 (over z), tp: 4 (over x, core).
Axes of the slice: x: 2, y: 2, z: 4, core: 2. Of those that a mesh axis runs over, the one named last changes fastest.
Arguments:
- query_rows: bfloat16 [3072, 2048], P(('grp', 'sp'), 'tp'), parts along dimension 0, may hold values from -6 to 6, as said below
- key_rows: bfloat16 [3072, 1024], P(('grp', 'sp'), 'tp'), parts along dimension 0, may hold values from -6 to 6, as said below
- value_rows: bfloat16 [3072, 1024], P(('grp', 'sp'), 'tp'), parts along dimension 0, may hold values from -15 to 15
- pool_input: bfloat16 [3072, 2048], P(('grp', 'sp'), 'tp'), parts along dimension 0, may hold values from -6 to 6
- log_gate_sums: float32 [3072, 16], P(('grp', 'sp'), 'tp'), parts along dimension 0, as said below
- query_gain: float32 [128], replicated, may hold values from 0.7 to 4.5, as said below
- key_gain: float32 [128], replicated, may hold values from 0.7 to 4.5, as said below
- pool_weight: bfloat16 [8, 256, 256], P('tp'), may hold values from -0.375 to 0.375
- pool_scale: float32 [2048], P('tp'), may hold values from 0.1 to 1.9
- attention_out: bfloat16 [2048, 4096], P('tp'), may hold values from -0.09375 to 0.09375
- pooling_out: bfloat16 [2048, 4096], P('tp'), may hold values from -0.09375 to 0.09375
Outputs:
- mixed_rows: bfloat16 [3072, 4096], P(('grp', 'sp', 'tp')), parts along dimension 0
There are 2 independent parts, one for each index of `grp`. A program takes and returns all parts, laid end to end along the dimension named above; an argument that names none is the same for every part. Nothing has to cross between parts.
Inputs may be any that keep to these rules, and one draw needn't show every extreme that they name: `query_rows`: normal entries; in some rows a query head's entries may equal its key head's entries of an earlier position. `key_rows`: normal entries. `log_gate_sums`: each column never rises from one position to the next. `query_gain`: Positive. `key_gain`: Positive.
All inputs are finite; a program needn't handle non-finite values.
Results may differ from a plain program's by a relative error of at most 0.014.
The roundings to bfloat16 on the way count: a program that leaves them out, or rounds other values in their place, can miss the bound.
Values may be sent and summed in bfloat16 or wider, within the bound.
A program may use at most 64 MiB of HBM per device.

v0:
```python
import math

import jax
import jax.numpy as jnp
from jax import lax
from jax.sharding import PartitionSpec as P

HEAD = 128
QUERY_HEADS = 16
KV_HEADS = 8
GROUP = 256
MAX_WINDOW = 16


epsilon = 1e-06
masked = -1e30


def from_behind(block, axis, distance):
    devices = range(lax.axis_size(axis))
    route = [(i - distance, i) for i in devices if i - distance in devices]
    return lax.ppermute(block, axis, route)


def head_norm(row_data, gain_vector, head_count):
    shaped = row_data.astype(jnp.float32).reshape(row_data.shape[0], head_count, -1)
    scaled = shaped * lax.rsqrt(jnp.mean(shaped * shaped, axis=-1, keepdims=True) + epsilon)
    return (scaled * gain_vector).astype(jnp.bfloat16)


def window_means(padded, length, first_pos, windows):
    rim_rows = padded.shape[0] - length
    window_sum = jnp.zeros((length,) + padded.shape[1:], jnp.float32)
    pooled = window_sum
    for lookback in range(rim_rows + 1):
        window_sum = window_sum + padded[rim_rows - lookback : rim_rows - lookback + length]
        window_size = lookback + 1
        if window_size >= 2 and window_size & window_size - 1 == 0:
            pooled = jnp.where((windows == window_size)[None, :, None], window_sum, pooled)
    positions = (first_pos + jnp.arange(length, dtype=jnp.int32)).astype(jnp.float32)
    counts = jnp.minimum(positions[:, None, None] + 1.0, windows.astype(jnp.float32)[None, :, None])
    return pooled / counts - padded[rim_rows:]


def attend_block(running, queries, query_gates, query_pos, pair_block, key_gates, key_pos):
    row_best, weight_sum, accumulated = running
    scores = jnp.einsum(
        "tkrd,skd->krts", queries, pair_block[0], preferred_element_type=jnp.float32
    )
    scores = scores * (1.0 / math.sqrt(HEAD)) + query_gates - key_gates
    allowed = key_pos[None, :] <= query_pos[:, None]
    scores = jnp.where(allowed, scores, masked)
    new_best = jnp.maximum(row_best, jnp.max(scores, axis=-1, keepdims=True))
    weights = jnp.where(allowed, jnp.exp(scores - new_best), 0.0)
    fading = jnp.exp(row_best - new_best)
    weight_sum = weight_sum * fading + jnp.sum(weights, axis=-1, keepdims=True)
    summed = jnp.einsum(
        "krts,skd->krtd",
        weights.astype(jnp.bfloat16),
        pair_block[1],
        preferred_element_type=jnp.float32,
    )
    return (new_best, weight_sum, accumulated * fading + summed)


def attend_piece(running, piece, queries, query_gates, query_pos, all_gates, valid):
    kv_here = queries.shape[1]
    ratio = queries.shape[2]
    piece_rows = piece.shape[1]
    block_rows = piece_rows
    while block_rows > 1024 and block_rows % 2 == 0:
        block_rows = block_rows // 2
    last_query = query_pos[query_pos.shape[0] - 1]

    def one_block(block_index, loop_state):
        first = block_index * block_rows

        def compute(state):
            pair_block = lax.dynamic_slice_in_dim(piece, block_index * block_rows, block_rows, 1)
            gate_block = lax.dynamic_slice_in_dim(all_gates, jnp.maximum(first, 0), block_rows, 0)
            gate_block = gate_block.T.reshape(kv_here, ratio, 1, block_rows)
            key_pos = first + jnp.arange(block_rows, dtype=jnp.int32)
            return attend_block(
                state, queries, query_gates, query_pos, pair_block, gate_block, key_pos
            )

        needed = jnp.logical_and(valid, first <= last_query)
        return lax.cond(needed, compute, lambda state: state, loop_state)

    return lax.fori_loop(0, piece_rows // block_rows, one_block, running)


def body(
    query_rows,
    key_rows,
    value_rows,
    pool_input,
    log_gate_sums,
    query_gain,
    key_gain,
    pool_weight,
    pool_scale,
    attention_out,
    pooling_out,
):
    length = query_rows.shape[0]
    kv_here = key_rows.shape[1] // HEAD
    ratio = QUERY_HEADS // KV_HEADS
    sp_index = lax.axis_index("sp")
    queries = head_norm(query_rows, query_gain, kv_here * ratio).reshape(
        length, kv_here, ratio, HEAD
    )
    pair = jnp.stack(
        [head_norm(key_rows, key_gain, kv_here), value_rows.reshape(length, kv_here, HEAD)]
    )
    all_gates = lax.all_gather(log_gate_sums, "sp", axis=0, tiled=True)
    query_gates = log_gate_sums.T.reshape(kv_here, ratio, length, 1)
    query_pos = sp_index * length + jnp.arange(length, dtype=jnp.int32)
    start_state = (
        jnp.full((kv_here, ratio, length, 1), masked, jnp.float32),
        jnp.zeros((kv_here, ratio, length, 1), jnp.float32),
        jnp.zeros((kv_here, ratio, length, HEAD), jnp.float32),
    )
    row_best, weight_sum, accumulated = attend_piece(
        start_state,
        lax.all_gather(pair, "sp", axis=1, tiled=True),
        queries,
        query_gates,
        query_pos,
        all_gates,
        jnp.int32(0) >= 0,
    )
    attended = (
        (accumulated / weight_sum)
        .transpose(2, 0, 1, 3)
        .reshape(length, kv_here * ratio * HEAD)
        .astype(jnp.bfloat16)
    )
    group_here = pool_input.shape[1] // GROUP
    rim = from_behind(pool_input[length - (MAX_WINDOW - 1) :], "sp", 1)
    padded = (
        jnp.concatenate([rim, pool_input])
        .astype(jnp.float32)
        .reshape(length + MAX_WINDOW - 1, group_here, GROUP)
    )
    levels = MAX_WINDOW.bit_length() - 1
    groups = lax.axis_index("tp") * group_here + jnp.arange(group_here, dtype=jnp.int32)
    windows = 2 ** (1 + groups % levels)
    pooled = window_means(padded, length, sp_index * length, windows).astype(jnp.bfloat16)
    mixing = jnp.einsum("tgc,gcd->tgd", pooled, pool_weight, preferred_element_type=jnp.float32)
    pool_mixed = (
        (mixing * pool_scale.reshape(group_here, GROUP))
        .astype(jnp.bfloat16)
        .reshape(length, group_here * GROUP)
    )
    total = jnp.dot(attended, attention_out, preferred_element_type=jnp.float32)
    return lax.psum_scatter(
        (total + jnp.dot(pool_mixed, pooling_out, preferred_element_type=jnp.float32)).astype(
            jnp.bfloat16
        ),
        "tp",
        scatter_dimension=0,
        tiled=True,
    )


def solution(mesh):
    return jax.shard_map(
        body,
        mesh=mesh,
        in_specs=(
            P(("grp", "sp"), "tp"),
            P(("grp", "sp"), "tp"),
            P(("grp", "sp"), "tp"),
            P(("grp", "sp"), "tp"),
            P(("grp", "sp"), "tp"),
            P(),
            P(),
            P("tp", None, None),
            P("tp"),
            P("tp", None),
            P("tp", None),
        ),
        out_specs=P(("grp", "sp", "tp"), None),
        check_vma=False,
    )
```

profile of v0, /device:TPU:28, one launch (start us, length us, event | category | flops | bytes accessed | tf_op | source)
XLA Modules:
  0.0 129.2 jit_solution(2364926939648079398)
XLA Ops:
  6.5 0.8 slice.110
  7.3 1.3 collective-permute-start
  8.6 1.1 copy.32
  9.8 1.1 copy.33
  11.7 0.8 pad_maximum_fusion
  12.5 1.2 copy.34
  16.1 0.9 copy.36
  17.1 13.5 %all_gather.7 = f32[1536,4]{0,1:T(4,128)S(1)} all-gather(f32[384,4]{0,1:T(4,128)S(1)} %copy-done.5), channel_id=1, replica_groups=mesh['grp'=2,'sp'=4,'tp'=4] {'sp'}, dimensions={0}, use_global_device_ids=true | all-gather | bytes 30720 | tf_op jit(solution)/shard_map/all_gather | solution.py:116
  30.7 3.6 %fusion.30 = (f32[384,512]{1,0:T(8,128)S(1)}, f32[384,512]{1,0:T(8,128)S(1)}, f32[384,512]{1,0:T(8,128)S(1)}, f32[384,512]{1,0:T(8,128)S(1)}, f32[384,512]{1,0:T...) fusion(f32[399,512]{1,0:T(8,128)S(1)} %maximum_convert_fusion), kind=kLoop, calls=%fused_computation.80 | loop fusion | bytes 25165824 | tf_op jit(solution)/shard_map/slice | solution.py:36
  34.2 4.8 %fusion.20 = bf16[2,384,256]{1,2,0:T(8,128)(2,1)S(1)} fusion(bf16[2,256,256]{2,1,0:T(8,128)(2,1)S(1)} %copy-done, f32[2,256]{1,0:T(2,128)S(1)} %mul.203, f32[48,2,8,256]{3,2,1,0:T(8,128)S(1)} %bitcast.209, f32[48,2,8,256]{3,2,1,0:T(8,128)S(1)} %bitcast.210, f32[48,2,8,256]{3,2,1,0:T(8,128)S(1)} %bitcast.211, f32[48,2,8,256]{3,2,1,0:T(8,128)S(1)} %bitcast.212, ...), kind=kOutput, calls=%fused_computation.29 | convolution fusion | flops 105381888 | bytes 13243400 | tf_op jit(solution)/shard_map/tgc,gcd->tgd/dot_general | solution.py:150
  39.0 10.9 %all-gather.2.cloned.1.call-done = bf16[2,1536,2,128]{1,3,2,0:T(8,128)(2,1)} async-done(((bf16[2,384,2,128]{1,3,2,0:T(8,128)(2,1)}), bf16[2,1536,2,128]{1,3,2,0:T(8,128)(2,1)}) %all-gather.2.cloned.1.call-update) | async-done | bytes 1572880 | tf_op jit(solution)/shard_map/all_gather | solution.py:126
  49.9 2.6 %copy.35 = bf16[2,1536,2,128]{3,1,2,0:T(8,128)(2,1)} copy(bf16[2,1536,2,128]{1,3,2,0:T(8,128)(2,1)} %all-gather.2.cloned.1.call-done) | data formatting | bytes 3145728
  52.6 22.5 %while.18 = (s32[]{:T(128)}, f32[2,2,384,1]{2,1,0,3:T(2,128)S(1)}, f32[2,2,384,1]{2,1,0,3:T(2,128)S(1)}, f32[2,2,384,128]{3,2,1,0:T(8,128)S(1)}, s32[]{:T(128)},...) while((s32[]{:T(128)}, f32[2,2,384,1]{2,1,0,3:T(2,128)S(1)}, ...), condition=%wide.region_7.8_spmd.clone, body=%wide.region_2.7_spmd.clone.sunk | while | flops 627086976 | bytes 37177752 | solution.py:90
  53.2 10.6 %conditional.3 = ((f32[2,2,384,1]{2,1,0,3:T(2,128)S(1)}, f32[2,2,384,1]{2,1,0,3:T(2,128)S(1)}, f32[2,2,384,128]{3,2,1,0:T(8,128)S(1)})) conditional(s32[]{:T(128)} %convert_element_type.104, (f32[2,2,384,1]{2,1,0,3:T(2,128)S(1)}, f32[2,2,384,1]{2,1,0,3:T(2,128)S(1)}, f32[2,2,384,128]{3,2,1,0:T(8,128)S(1)}) %tuple.62, (s32[]{:T(128)}, s32[]{:T(128)}, ...), branch_computations={%region_3.0_spmd, %region_4.6_spmd} | conditional | flops 627086976 | bytes 37175960 | solution.py:88
  53.6 3.9 %fusion.6 = (f32[2,2,384]{2,1,0:T(2,128)S(1)}, f32[2,768,384,2]{2,1,3,0:T(8,128)}) fusion(f32[2,2,768]{2,1,0:T(2,128)S(1)} %sub.6, f32[2,2,384]{2,1,0:T(2,128)S(1)} %bitcast.231, pred[384,768]{0,1:T(8,128)(4,1)S(1)} %broadcast_compare_fusion, bf16[384,2,2,128]{3,0,2,1:T(8,128)(2,1)S(1)} %get-tuple-element.199, ...), kind=kOutput, calls=%fused_computation.7 | convolution fusion | flops 307886592 | bytes 5824516 | tf_op jit(solution)/shard_map/while/body/eval_jaxpr/cond/branch_1_fun/tkrd,skd->krts/dot_general | solution.py:47
  57.6 4.6 %fusion.10 = f32[2,2,384,128]{3,2,1,0:T(8,128)S(1)} fusion(f32[2,768,384,2]{2,1,3,0:T(8,128)} %get-tuple-element.284, f32[2,2,384]{2,1,0:T(2,128)S(1)} %bitcast.224, f32[2,2,768]{2,1,0:T(2,128)S(1)} %sub.6, f32[2,2,384]{2,1,0:T(2,128)S(1)} %bitcast.232, pred[384,768]{0,1:T(8,128)(4,1)S(1)} %broadcast_compare_fusion, ...), kind=kOutput, calls=%fused_computation.10 | convolution fusion | flops 310640640 | bytes 7010312 | tf_op jit(solution)/shard_map/while/body/eval_jaxpr/cond/branch_1_fun/krts,skd->krtd/dot_general | solution.py:57
  62.2 1.6 %fusion.5 = f32[2,2,384]{2,1,0:T(2,128)S(1)} fusion(f32[2,768,384,2]{2,1,3,0:T(8,128)S(1)} %copy-done.1, f32[2,2,384]{2,1,0:T(2,128)S(1)} %bitcast.225, f32[2,2,768]{2,1,0:T(2,128)S(1)} %sub.6, f32[2,2,384]{2,1,0:T(2,128)S(1)} %bitcast.233, pred[384,768]{0,1:T(8,128)(4,1)S(1)} %broadcast_compare_fusion), kind=kLoop, calls=%fused_computation.6 | loop fusion | flops 8256000 | bytes 5044224 | tf_op jit(solution)/shard_map/while/body/eval_jaxpr/cond/branch_1_fun/reduce_sum | solution.py:56
  64.5 10.6 %conditional.3 = ((f32[2,2,384,1]{2,1,0,3:T(2,128)S(1)}, f32[2,2,384,1]{2,1,0,3:T(2,128)S(1)}, f32[2,2,384,128]{3,2,1,0:T(8,128)S(1)})) conditional(s32[]{:T(128)} %convert_element_type.104, (f32[2,2,384,1]{2,1,0,3:T(2,128)S(1)}, f32[2,2,384,1]{2,1,0,3:T(2,128)S(1)}, f32[2,2,384,128]{3,2,1,0:T(8,128)S(1)}) %tuple.62, (s32[]{:T(128)}, s32[]{:T(128)}, ...), branch_computations={%region_3.0_spmd, %region_4.6_spmd} | conditional | flops 627086976 | bytes 37175960 | solution.py:88
  64.8 3.9 %fusion.6 = (f32[2,2,384]{2,1,0:T(2,128)S(1)}, f32[2,768,384,2]{2,1,3,0:T(8,128)}) fusion(f32[2,2,768]{2,1,0:T(2,128)S(1)} %sub.6, f32[2,2,384]{2,1,0:T(2,128)S(1)} %bitcast.231, pred[384,768]{0,1:T(8,128)(4,1)S(1)} %broadcast_compare_fusion, bf16[384,2,2,128]{3,0,2,1:T(8,128)(2,1)S(1)} %get-tuple-element.199, ...), kind=kOutput, calls=%fused_computation.7 | convolution fusion | flops 307886592 | bytes 5824516 | tf_op jit(solution)/shard_map/while/body/eval_jaxpr/cond/branch_1_fun/tkrd,skd->krts/dot_general | solution.py:47
  68.8 4.6 %fusion.10 = f32[2,2,384,128]{3,2,1,0:T(8,128)S(1)} fusion(f32[2,768,384,2]{2,1,3,0:T(8,128)} %get-tuple-element.284, f32[2,2,384]{2,1,0:T(2,128)S(1)} %bitcast.224, f32[2,2,768]{2,1,0:T(2,128)S(1)} %sub.6, f32[2,2,384]{2,1,0:T(2,128)S(1)} %bitcast.232, pred[384,768]{0,1:T(8,128)(4,1)S(1)} %broadcast_compare_fusion, ...), kind=kOutput, calls=%fused_computation.10 | convolution fusion | flops 310640640 | bytes 7010312 | tf_op jit(solution)/shard_map/while/body/eval_jaxpr/cond/branch_1_fun/krts,skd->krtd/dot_general | solution.py:57
  73.4 1.6 %fusion.5 = f32[2,2,384]{2,1,0:T(2,128)S(1)} fusion(f32[2,768,384,2]{2,1,3,0:T(8,128)S(1)} %copy-done.1, f32[2,2,384]{2,1,0:T(2,128)S(1)} %bitcast.225, f32[2,2,768]{2,1,0:T(2,128)S(1)} %sub.6, f32[2,2,384]{2,1,0:T(2,128)S(1)} %bitcast.233, pred[384,768]{0,1:T(8,128)(4,1)S(1)} %broadcast_compare_fusion), kind=kLoop, calls=%fused_computation.6 | loop fusion | flops 8256000 | bytes 5044224 | tf_op jit(solution)/shard_map/while/body/eval_jaxpr/cond/branch_1_fun/reduce_sum | solution.py:56
  75.5 4.2 %fusion.31 = f32[384,4096]{1,0:T(8,128)S(1)} fusion(bf16[384,512]{0,1:T(8,128)(2,1)S(1)} %bitcast.228, bf16[512,4096]{1,0:T(8,128)(2,1)} %param.24), kind=kOutput, calls=%fused_computation.81 | convolution fusion | flops 1610612736 | bytes 10878976 | tf_op jit(solution)/shard_map/dot_general | solution.py:156
  79.7 3.7 %add_convert_fusion = bf16[384,4096]{1,0:T(8,128)(2,1)} fusion(f32[384,4096]{1,0:T(8,128)S(1)} %fusion.31, bf16[384,512]{0,1:T(8,128)(2,1)S(1)} %bitcast.227, bf16[512,4096]{1,0:T(8,128)(2,1)S(1)} %copy-done.2), kind=kOutput, calls=%fused_computation.27 | convolution fusion | flops 1613758464 | bytes 14024704 | tf_op jit(solution)/shard_map/dot_general | solution.py:158
  83.4 39.0 %reduce-scatter.2.cloned.1.call-done = bf16[96,4096]{1,0:T(8,128)(2,1)} async-done(((bf16[384,4096]{1,0:T(8,128)(2,1)}), bf16[96,4096]{1,0:T(8,128)(2,1)}) %reduce-scatter.2.cloned.1.call-update) | async-done | bytes 786448 | tf_op jit(solution)/shard_map/reduce_scatter | solution.py:157
  (59 shorter events, 4.5 us)
Async XLA Ops:
  6.5 27.7 %copy-start = (bf16[2,256,256]{2,1,0:T(8,128)(2,1)S(1)}, bf16[2,256,256]{2,1,0:T(8,128)(2,1)}, u32[]{:S(2)}) copy-start(bf16[2,256,256]{2,1,0:T(8,128)(2,1)} %param.22) | copy-start | bytes 786436
  6.5 24.0 %copy-start.3 = (bf16[384,512]{1,0:T(8,128)(2,1)S(1)}, bf16[384,512]{1,0:T(8,128)(2,1)}, u32[]{:S(2)}) copy-start(bf16[384,512]{1,0:T(8,128)(2,1)} %param.18) | copy-start | bytes 1179652
  6.5 10.5 %copy-start.5 = (f32[384,4]{0,1:T(4,128)S(1)}, f32[384,4]{0,1:T(4,128)}, u32[]{:S(2)}) copy-start(f32[384,4]{0,1:T(4,128)} %param.19) | copy-start | bytes 18436
  6.5 43.4 %all-gather.2.cloned.1.call-start = ((), (), s32[]{:S(2)}) async-start(), calls=%async_computation.1 | async-start | bytes 1966080 | tf_op jit(solution)/shard_map/all_gather | solution.py:126
  7.3 23.2 %collective-permute-start = (bf16[15,512]{1,0:T(8,128)(2,1)S(1)}, bf16[15,512]{1,0:T(8,128)(2,1)S(1)}, u32[]{:S(2)}, u32[]{:S(2)}) collective-permute-start(bf16[15,512]{1,0:T(8,128)(2,1)S(1)} %slice.110), channel_id=1, source_target_pairs={{0,4},{4,8},{8,12},{1,5},{5,9},{9,13},{2,6},{6,10},{10,14},{3,7},{... | collective-permute-start | bytes 46088 | tf_op jit(solution)/shard_map/ppermute | solution.py:22
  12.5 109.9 %reduce-scatter.2.cloned.1.call-start = ((), (), s32[]{:S(2)}) async-start(), calls=%async_computation.2 | async-start | bytes 3932160 | tf_op jit(solution)/shard_map/reduce_scatter | solution.py:157
  34.2 18.4 %copy-start.4 = (bf16[384,2,2,128]{3,0,2,1:T(8,128)(2,1)S(1)}, bf16[384,2,2,128]{3,0,2,1:T(8,128)(2,1)}, u32[]{:S(2)}) copy-start(bf16[384,2,2,128]{3,0,2,1:T(8,128)(2,1)} %copy.36) | copy-start | bytes 1179652
  57.6 4.6 %copy-start.1 = (f32[2,768,384,2]{2,1,3,0:T(8,128)S(1)}, f32[2,768,384,2]{2,1,3,0:T(8,128)}, u32[]{:S(2)}) copy-start(f32[2,768,384,2]{2,1,3,0:T(8,128)} %get-tuple-element.284) | copy-start | bytes 14155780 | tf_op jit(solution)/shard_map/while/body/eval_jaxpr/cond
  68.8 4.6 %copy-start.1 = (f32[2,768,384,2]{2,1,3,0:T(8,128)S(1)}, f32[2,768,384,2]{2,1,3,0:T(8,128)}, u32[]{:S(2)}) copy-start(f32[2,768,384,2]{2,1,3,0:T(8,128)} %get-tuple-element.284) | copy-start | bytes 14155780 | tf_op jit(solution)/shard_map/while/body/eval_jaxpr/cond
  75.5 4.2 %copy-start.2 = (bf16[512,4096]{1,0:T(8,128)(2,1)S(1)}, bf16[512,4096]{1,0:T(8,128)(2,1)}, u32[]{:S(2)}) copy-start(bf16[512,4096]{1,0:T(8,128)(2,1)} %param.25) | copy-start | bytes 12582916
Sparse Core Ops, SparseCore 0:
  12.6 37.2 all-gather.1
  83.6 38.7 reduce-scatter.1
where the time goes:
time: 131 us; the launch traced here: 129 us
  waiting for transfers between devices  49.9 us (38%)
  matrix products  29.7 us (23%)
  between operations  13.6 us (10%)
  blocking collectives  13.5 us (10%)
  local copies, waits for them, and re-layouts  13.1 us (10%)
  other arithmetic  6.66 us (5%)
  loops' own time  1.39 us (1%)
  starting transfers between devices  1.32 us (1%)
    reduce_scatter x1, waiting for transfers between devices, body(): lax.psum_scatter((total + jnp.dot(pool_mixed, pooling_out, preferred_elem...  39 us
    all_gather x1, blocking collectives, body(): all_gates = lax.all_gather(log_gate_sums, 'sp', axis=0, tiled=True)  13.5 us
    all_gather x1, waiting for transfers between devices, body(): lax.all_gather(pair, 'sp', axis=1, tiled=True)  10.9 us
    dot_general x2, matrix products, attend_block(): jnp.einsum('krts,skd->krtd', weights.astype(jnp.bfloat16), pair_block[1],...  9.18 us
    dot_general x2, matrix products, attend_block(): jnp.einsum('tkrd,skd->krts', queries, pair_block[0], preferred_element_ty...  7.89 us
    unnamed x15, local copies, waits for them, and re-layouts  6.93 us
    dot_general x1, matrix products, body(): jnp.einsum('tgc,gcd->tgd', pooled, pool_weight, preferred_element_type=jn...  4.76 us
    dot_general x1, matrix products, body(): total = jnp.dot(attended, attention_out, preferred_element_type=jnp.float32)  4.23 us
  transfers between devices with their start and end apart: 3, of which 2 were waited for; matrix products, arithmetic and copies ran while one was open for 13% of the time, Pallas kernels for 0%

commit v1 on v0

v1 whole, which is shorter than its diff:
```python
import functools
import math

import jax
import jax.numpy as jnp
from jax import lax
from jax.experimental import pallas as pl
from jax.experimental.pallas import tpu as pltpu
from jax.sharding import PartitionSpec as P

HEAD = 128
QUERY_HEADS = 16
KV_HEADS = 8
GROUP = 256
MAX_WINDOW = 16
RATIO = QUERY_HEADS // KV_HEADS
RIM = 16
CHUNK = 512

epsilon = 1e-06
masked = -1e30
MESH = pl.DeviceIdType.MESH
f32 = jnp.float32
bf16 = jnp.bfloat16


def normed(rows, gain):
    rows = rows.astype(f32)
    scale = lax.rsqrt(jnp.mean(rows * rows, axis=-1, keepdims=True) + epsilon)
    return (rows * scale * gain).astype(bf16)


def kernel(
    n_sp,
    n_tp,
    q_hbm,
    k_hbm,
    v_hbm,
    p_hbm,
    gates,
    q_gain,
    k_gain,
    pool_weight,
    pool_scale,
    wa_hbm,
    wp_hbm,
    out_hbm,
    q_raw,
    k_raw,
    kv,
    gate_rows,
    qn,
    best,
    sums,
    acc,
    padded,
    act,
    weights,
    part,
    pair_in,
    x_out,
    x_in,
    own,
    out_buf,
    in_sems,
    w_sems,
    kv_send,
    kv_recv,
    rim_sems,
    d_send,
    d_recv,
    x_send,
    x_recv,
    out_sems,
):
    length = q_raw.shape[0]
    kv_here = k_raw.shape[1] // HEAD
    heads = kv_here * RATIO
    group_here = padded.shape[1] // GROUP
    att_w = heads * HEAD
    n_x = n_tp // 2
    rows_out = length // n_tp
    chip_rows = 2 * rows_out
    chunks = weights.shape[0]
    gate_item = 2 * kv_here

    me = lax.axis_index("sp")
    tp = lax.axis_index("tp")
    x = tp // 2
    c = tp % 2
    partner = x * 2 + (1 - c)
    has_next = me < n_sp - 1
    has_prev = me > 0

    def across(dx):
        return lax.rem(x + dx, n_x) * 2 + c

    ins = [
        pltpu.make_async_copy(k_hbm, k_raw, in_sems.at[0]),
        pltpu.make_async_copy(p_hbm, padded.at[pl.ds(RIM, length)], in_sems.at[1]),
        pltpu.make_async_copy(q_hbm, q_raw, in_sems.at[2]),
    ]
    for h in range(kv_here):
        ins.append(
            pltpu.make_async_copy(
                v_hbm.at[:, pl.ds(h * HEAD, HEAD)], kv.at[me, h, 1], in_sems.at[3 + h]
            )
        )
    for copy in ins:
        copy.start()
    loads = []
    for j in range(chunks):
        cols = pl.ds(j * CHUNK, CHUNK)
        loads.append(
            pltpu.make_async_copy(
                wa_hbm.at[:, cols], weights.at[j, pl.ds(0, att_w)], w_sems.at[2 * j]
            )
        )
        loads.append(
            pltpu.make_async_copy(
                wp_hbm.at[:, cols],
                weights.at[j, pl.ds(att_w, weights.shape[1] - att_w)],
                w_sems.at[2 * j + 1],
            )
        )

    barrier = pltpu.get_barrier_semaphore()

    def greet(where):
        pl.semaphore_signal(barrier, inc=1, device_id=where, device_id_type=MESH)

    @pl.when(has_next)
    def _():
        greet({"sp": me + 1})

    @pl.when(has_prev)
    def _():
        greet({"sp": me - 1})

    greet({"tp": partner})
    for dx in range(1, n_x):
        greet({"tp": across(dx)})

    k_scale = k_gain[...]
    q_scale = q_gain[...]
    ins[0].wait()
    for h in range(kv_here):
        kv[me, h, 0] = normed(k_raw[:, h * HEAD : (h + 1) * HEAD], k_scale)
    on_diagonal = lax.broadcasted_iota(jnp.int32, (length, length), 0) == (
        lax.broadcasted_iota(jnp.int32, (length, length), 1)
    )
    for i in range(heads):
        gate_rows[me, pl.ds(i, 1)] = jnp.sum(
            jnp.where(on_diagonal, gates[:, i : i + 1], 0.0), axis=0, keepdims=True
        )
    for copy in ins[3:]:
        copy.wait()
    ins[1].wait()

    pl.semaphore_wait(barrier, n_x + has_next.astype(jnp.int32) + has_prev.astype(jnp.int32))

    after = jnp.minimum(me + 1, n_sp - 1)

    def hand_on(slot, item):
        if item == gate_item:
            block = gate_rows.at[slot]
        else:
            block = kv.at[slot, item // 2, 1 - item % 2]
        return pltpu.make_async_remote_copy(
            src_ref=block,
            dst_ref=block,
            send_sem=kv_send.at[slot, item],
            recv_sem=kv_recv.at[slot, item],
            device_id={"sp": after},
            device_id_type=MESH,
        )

    rim_copy = pltpu.make_async_remote_copy(
        src_ref=padded.at[pl.ds(length, RIM)],
        dst_ref=padded.at[pl.ds(0, RIM)],
        send_sem=rim_sems.at[0],
        recv_sem=rim_sems.at[1],
        device_id={"sp": after},
        device_id_type=MESH,
    )

    @pl.when(has_next)
    def _():
        hand_on(me, gate_item).start()
        for item in range(gate_item):
            hand_on(me, item).start()
        rim_copy.start()

    for copy in loads:
        copy.start()

    ins[2].wait()
    for i in range(heads):
        qn[i] = normed(q_raw[:, i * HEAD : (i + 1) * HEAD], q_scale)

    def score_of(i, slot):
        scores = lax.dot_general(
            qn[i], kv[slot, i // RATIO, 0], (((1,), (1,)), ((), ())), preferred_element_type=f32
        )
        drop = gates[:, i : i + 1] - gate_rows[slot, pl.ds(i, 1)]
        return scores * (1.0 / math.sqrt(HEAD)) + drop

    allowed = lax.broadcasted_iota(jnp.int32, (length, length), 1) <= (
        lax.broadcasted_iota(jnp.int32, (length, length), 0)
    )
    for i in range(heads):
        scores = jnp.where(allowed, score_of(i, me), masked)
        top = jnp.max(scores, axis=-1, keepdims=True)
        shares = jnp.where(allowed, jnp.exp(scores - top), 0.0)
        best[i] = top
        sums[i] = jnp.sum(shares, axis=-1, keepdims=True)
        acc[i] = jnp.dot(shares.astype(bf16), kv[me, i // RATIO, 1], preferred_element_type=f32)

    def attend(i, slot):
        scores = score_of(i, slot)
        old = best[i]
        top = jnp.maximum(old, jnp.max(scores, axis=-1, keepdims=True))
        shares = jnp.exp(scores - top)
        fading = jnp.exp(old - top)
        best[i] = top
        sums[i] = sums[i] * fading + jnp.sum(shares, axis=-1, keepdims=True)
        acc[i] = acc[i] * fading + jnp.dot(
            shares.astype(bf16), kv[slot, i // RATIO, 1], preferred_element_type=f32
        )

    @pl.when(has_prev)
    def _():
        rim_copy.wait_recv()

    @pl.when(jnp.logical_not(has_prev))
    def _():
        padded[pl.ds(0, RIM)] = jnp.zeros((RIM, padded.shape[1]), bf16)

    levels = MAX_WINDOW.bit_length() - 1
    first = me * length
    position = (first + lax.broadcasted_iota(jnp.int32, (length, 1), 0)).astype(f32)
    for g in range(group_here):
        cols = slice(g * GROUP, (g + 1) * GROUP)
        level = (tp * group_here + g) % levels
        rows = padded[:, cols].astype(f32)
        running = rows
        window_sum = None
        for step in range(levels):
            running = running + pltpu.roll(running, 1 << step, 0)
            if window_sum is None:
                window_sum = running
            else:
                window_sum = jnp.where(level >= step, running, window_sum)
        window = lax.shift_left(jnp.int32(2), level).astype(f32)
        counts = jnp.minimum(position + 1.0, window)
        pooled = (window_sum[RIM:] / counts - rows[RIM:]).astype(bf16)
        mixing = jnp.dot(pooled, pool_weight[g], preferred_element_type=f32)
        act[:, att_w + g * GROUP : att_w + (g + 1) * GROUP] = (
            mixing * pool_scale[:, cols]
        ).astype(bf16)

    def one_step(step, carry):
        slot = me - step

        def take(item):
            hand_on(slot, item).wait_recv()

            @pl.when(has_next)
            def _():
                hand_on(slot, item).start()

        take(gate_item)
        for h in range(kv_here):
            take(2 * h)
            take(2 * h + 1)
            for r in range(RATIO):
                attend(h * RATIO + r, slot)
        return carry

    lax.fori_loop(1, me + 1, one_step, 0)
    for i in range(heads):
        act[:, i * HEAD : (i + 1) * HEAD] = (acc[i] / sums[i]).astype(bf16)

    for copy in loads:
        copy.wait()

    def pair_copy(dx, j):
        return pltpu.make_async_remote_copy(
            src_ref=part.at[dx, j, pl.ds(pl.multiple_of((1 - c) * rows_out, 16), rows_out)],
            dst_ref=pair_in.at[dx, j],
            send_sem=d_send.at[dx, j],
            recv_sem=d_recv.at[dx, j],
            device_id={"tp": partner},
            device_id_type=MESH,
        )

    def x_copy(dx, j):
        return pltpu.make_async_remote_copy(
            src_ref=x_out.at[dx - 1, j],
            dst_ref=x_in.at[dx - 1, j],
            send_sem=x_send.at[dx - 1, j],
            recv_sem=x_recv.at[dx - 1, j],
            device_id={"tp": across(dx)},
            device_id_type=MESH,
        )

    def project(dx, j):
        top_row = pl.multiple_of(lax.rem(x + dx, n_x) * chip_rows, 16)
        part[dx, j] = jnp.dot(
            act[pl.ds(top_row, chip_rows)], weights[j], preferred_element_type=f32
        ).astype(bf16)
        pair_copy(dx, j).start()

    def pair_sum(dx, j):
        pair_copy(dx, j).wait_recv()
        mine = part[dx, j, pl.ds(pl.multiple_of(c * rows_out, 16), rows_out)]
        return mine.astype(f32) + pair_in[dx, j].astype(f32)

    for dx in list(range(1, n_x)) + [0]:

        def finish(j, dx=dx):
            total = pair_sum(dx, j)
            if dx == 0:
                own[j] = total
            else:
                x_out[dx - 1, j] = total.astype(bf16)
                x_copy(dx, j).start()

        def one_chunk(j, carry, dx=dx, finish=finish):
            project(dx, j)

            @pl.when(j > 0)
            def _():
                finish(j - 1)

            return carry

        lax.fori_loop(0, chunks, one_chunk, 0)
        finish(chunks - 1)

    def out_copy(j):
        return pltpu.make_async_copy(
            out_buf.at[j],
            out_hbm.at[:, pl.ds(pl.multiple_of(j * CHUNK, CHUNK), CHUNK)],
            out_sems.at[j],
        )

    def last(j, carry):
        total = own[j]
        for dx in range(1, n_x):
            x_copy(dx, j).wait_recv()
            total = total + x_in[dx - 1, j].astype(f32)
        out_buf[j] = total.astype(bf16)
        out_copy(j).start()
        return carry

    lax.fori_loop(0, chunks, last, 0)

    def drain(j, carry):
        out_copy(j).wait()
        for dx in range(n_x):
            pair_copy(dx, j).wait_send()
            if dx:
                x_copy(dx, j).wait_send()
        return carry

    lax.fori_loop(0, chunks, drain, 0)

    @pl.when(has_next)
    def _():
        rim_copy.wait_send()

        def sent(slot, carry):
            for item in range(gate_item + 1):
                hand_on(slot, item).wait_send()
            return carry

        lax.fori_loop(0, me + 1, sent, 0)


def body(n_sp, n_tp, q, k, v, p, gates, q_gain, k_gain, pool_weight, pool_scale, wa, wp):
    length = q.shape[0]
    kv_here = k.shape[1] // HEAD
    heads = kv_here * RATIO
    width = wa.shape[1]
    n_x = n_tp // 2
    rows_out = length // n_tp
    chunks = width // CHUNK
    depth = wa.shape[0] + wp.shape[0]
    items = 2 * kv_here + 1
    dma = pltpu.SemaphoreType.DMA
    hbm = pl.BlockSpec(memory_space=pl.ANY)
    vmem = pl.BlockSpec(memory_space=pltpu.VMEM)
    far = max(n_x - 1, 1)
    return pl.pallas_call(
        functools.partial(kernel, n_sp, n_tp),
        out_shape=jax.ShapeDtypeStruct((rows_out, width), bf16),
        in_specs=[hbm] * 4 + [vmem] * 5 + [hbm] * 2,
        out_specs=hbm,
        scratch_shapes=[
            pltpu.VMEM(q.shape, bf16),
            pltpu.VMEM(k.shape, bf16),
            pltpu.VMEM((n_sp, kv_here, 2, length, HEAD), bf16),
            pltpu.VMEM((n_sp, 8, length), f32),
            pltpu.VMEM((heads, length, HEAD), bf16),
            pltpu.VMEM((heads, length, 1), f32),
            pltpu.VMEM((heads, length, 1), f32),
            pltpu.VMEM((heads, length, HEAD), f32),
            pltpu.VMEM((length + RIM, p.shape[1]), bf16),
            pltpu.VMEM((length, depth), bf16),
            pltpu.VMEM((chunks, depth, CHUNK), bf16),
            pltpu.VMEM((n_x, chunks, 2 * rows_out, CHUNK), bf16),
            pltpu.VMEM((n_x, chunks, rows_out, CHUNK), bf16),
            pltpu.VMEM((far, chunks, rows_out, CHUNK), bf16),
            pltpu.VMEM((far, chunks, rows_out, CHUNK), bf16),
            pltpu.VMEM((chunks, rows_out, CHUNK), f32),
            pltpu.VMEM((chunks, rows_out, CHUNK), bf16),
            dma((3 + kv_here,)),
            dma((2 * chunks,)),
            dma((n_sp, items)),
            dma((n_sp, items)),
            dma((2,)),
            dma((n_x, chunks)),
            dma((n_x, chunks)),
            dma((far, chunks)),
            dma((far, chunks)),
            dma((chunks,)),
        ],
        compiler_params=pltpu.CompilerParams(
            collective_id=0, has_side_effects=True, vmem_limit_bytes=60 * 1024 * 1024
        ),
        name="mixer",
    )(
        q,
        k,
        v,
        p,
        gates,
        q_gain.reshape(1, -1),
        k_gain.reshape(1, -1),
        pool_weight,
        pool_scale.reshape(1, -1),
        wa,
        wp,
    )


def solution(mesh):
    return jax.shard_map(
        functools.partial(body, mesh.shape["sp"], mesh.shape["tp"]),
        mesh=mesh,
        in_specs=(
            P(("grp", "sp"), "tp"),
            P(("grp", "sp"), "tp"),
            P(("grp", "sp"), "tp"),
            P(("grp", "sp"), "tp"),
            P(("grp", "sp"), "tp"),
            P(),
            P(),
            P("tp", None, None),
            P("tp"),
            P("tp", None),
            P("tp", None),
        ),
        out_specs=P(("grp", "sp", "tp"), None),
        check_vma=False,
    )
```

time: 131 us -> 59 us (0.45)
  Pallas kernels: 0 us -> 54.9 us
  waiting for transfers between devices: 49.9 us -> 0 us
  matrix products: 29.7 us -> 0 us
  between operations: 13.6 us -> 0.01 us
  blocking collectives: 13.5 us -> 0 us
  local copies, waits for them, and re-layouts: 13.1 us -> 3.57 us
  other arithmetic: 6.66 us -> 0 us
  loops' own time: 1.39 us -> 0 us
  starting transfers between devices: 1.32 us -> 0 us
    pallas_call x0 -> x1, Pallas kernels: none -> 54.9 us  [body(): pl.pallas_call(functools.partial(kernel, n_sp, n_tp), out_shape=jax.Shape...]
    reduce_scatter x1 -> x0, waiting for transfers between devices: 39 us -> none  [body(): lax.psum_scatter((total + jnp.dot(pool_mixed, pooling_out, preferred_elem...]
    dot_general x7 -> x0, matrix products: 29.7 us -> none  [the longest x2 9.18 us: attend_block(): jnp.einsum('krts,skd->krtd', weights.astype(jnp.bfloat16), pair_block[1],...]
    all_gather x1 -> x0, blocking collectives: 13.5 us -> none  [body(): all_gates = lax.all_gather(log_gate_sums, 'sp', axis=0, tiled=True)]
    all_gather x1 -> x0, waiting for transfers between devices: 10.9 us -> none  [body(): lax.all_gather(pair, 'sp', axis=1, tiled=True)]
    slice x3 -> x0, local copies, waits for them, and re-layouts: 4.92 us -> none  [the longest x1 3.55 us: window_means(): padded[rim_rows - lookback:rim_rows - lookback + length]]
    reduce_sum x4 -> x0, other arithmetic: 3.45 us -> none  [the longest x2 3.3 us: attend_block(): weight_sum = weight_sum * fading + jnp.sum(weights, axis=-1, keepdims=True)]
    unnamed x15 -> x2, local copies, waits for them, and re-layouts: 6.93 us -> 3.57 us
  transfers between devices with their start and end apart: 3 -> 0, of which waited for: 2 -> 0; matrix products, arithmetic and copies ran while one was open for 13% -> 0% of each run, Pallas kernels for 0% -> 0%
where the time goes in v1:
time: 59 us; the launch traced here: 58.4 us
  Pallas kernels  54.9 us (93%)
  local copies, waits for them, and re-layouts  3.57 us (6%)
    pallas_call x1, Pallas kernels, body(): pl.pallas_call(functools.partial(kernel, n_sp, n_tp), out_shape=jax.Shape...  54.9 us
    unnamed x2, local copies, waits for them, and re-layouts  3.57 us

profile of v1, /device:TPU:28, one launch (start us, length us, event | category | flops | bytes accessed | tf_op | source)
XLA Modules:
  0.0 58.4 jit_solution(16263573474321050285)
XLA Ops:
  0.0 1.5 %copy.12.gates = f32[384,4]{1,0:T(8,128)} copy(f32[384,4]{0,1:T(4,128)} %param.15) | data formatting | bytes 12288 | tf_op args[4]
  1.5 54.9 %mixer.1 = bf16[96,4096]{1,0:T(8,128)(2,1)} custom-call(bf16[384,512]{1,0:T(8,128)(2,1)} %q_hbm.1, bf16[384,256]{1,0:T(8,128)(2,1)} %k_hbm.1, bf16[384,256]{1,0:T(8,128)(2,1)} %v_hbm.1, bf16[384,512]{1,0:T(8,128)(2,1)} %p_hbm.1, f32[384,4]{1,0:T(8,128)} %copy.12.gates, f32[1,128]{1,0:T(1,128)} %bitcast.4, f32[1,128]{1,0:T(1,128)} %bitcast.5, ...), custom_call_target="tpu_custom_call" | custom-call | tf_op jit(solution)/shard_map/mixer/pallas_call | solution.py:395
  56.4 2.1 %copy.14 = bf16[96,4096]{1,0:T(8,128)(2,1)} copy(bf16[96,4096]{1,0:T(8,128)(2,1)} %mixer.1) | data formatting | bytes 1572864

commit v2 on v1

--- a/solution.py
+++ b/solution.py
@@ -15,7 +15,7 @@
 MAX_WINDOW = 16
 RATIO = QUERY_HEADS // KV_HEADS
 RIM = 16
-CHUNK = 512
+CHUNK = 256
 
 epsilon = 1e-06
 masked = -1e30
@@ -49,6 +49,7 @@
     k_raw,
     kv,
     gate_rows,
+    gate_cols,
     qn,
     best,
     sums,
@@ -146,13 +147,6 @@
     ins[0].wait()
     for h in range(kv_here):
         kv[me, h, 0] = normed(k_raw[:, h * HEAD : (h + 1) * HEAD], k_scale)
-    on_diagonal = lax.broadcasted_iota(jnp.int32, (length, length), 0) == (
-        lax.broadcasted_iota(jnp.int32, (length, length), 1)
-    )
-    for i in range(heads):
-        gate_rows[me, pl.ds(i, 1)] = jnp.sum(
-            jnp.where(on_diagonal, gates[:, i : i + 1], 0.0), axis=0, keepdims=True
-        )
     for copy in ins[3:]:
         copy.wait()
     ins[1].wait()
@@ -161,13 +155,13 @@
 
     after = jnp.minimum(me + 1, n_sp - 1)
 
-    def hand_on(slot, item):
+    def hand_on(slot, item, own_gates=False):
         if item == gate_item:
             block = gate_rows.at[slot]
         else:
-            block = kv.at[slot, item // 2, 1 - item % 2]
+            block = kv.at[slot, item // 2, item % 2]
         return pltpu.make_async_remote_copy(
-            src_ref=block,
+            src_ref=gates if own_gates else block,
             dst_ref=block,
             send_sem=kv_send.at[slot, item],
             recv_sem=kv_recv.at[slot, item],
@@ -186,10 +180,11 @@
 
     @pl.when(has_next)
     def _():
-        hand_on(me, gate_item).start()
-        for item in range(gate_item):
+        rim_copy.start()
+        hand_on(me, 0).start()
+        hand_on(me, gate_item, True).start()
+        for item in range(1, gate_item):
             hand_on(me, item).start()
-        rim_copy.start()
 
     for copy in loads:
         copy.start()
@@ -198,35 +193,65 @@
     for i in range(heads):
         qn[i] = normed(q_raw[:, i * HEAD : (i + 1) * HEAD], q_scale)
 
-    def score_of(i, slot):
+    on_diagonal = lax.broadcasted_iota(jnp.int32, (length, length), 0) == (
+        lax.broadcasted_iota(jnp.int32, (length, length), 1)
+    )
+    for i in range(heads):
+        gate_cols[i] = jnp.sum(
+            jnp.where(on_diagonal, gates[pl.ds(i, 1)], 0.0), axis=1, keepdims=True
+        )
+
+    def score_of(i, slot, key_gates):
         scores = lax.dot_general(
             qn[i], kv[slot, i // RATIO, 0], (((1,), (1,)), ((), ())), preferred_element_type=f32
         )
-        drop = gates[:, i : i + 1] - gate_rows[slot, pl.ds(i, 1)]
+        drop = gate_cols[i] - key_gates
         return scores * (1.0 / math.sqrt(HEAD)) + drop
 
     allowed = lax.broadcasted_iota(jnp.int32, (length, length), 1) <= (
         lax.broadcasted_iota(jnp.int32, (length, length), 0)
     )
     for i in range(heads):
-        scores = jnp.where(allowed, score_of(i, me), masked)
+        scores = jnp.where(allowed, score_of(i, me, gates[pl.ds(i, 1)]), masked)
         top = jnp.max(scores, axis=-1, keepdims=True)
         shares = jnp.where(allowed, jnp.exp(scores - top), 0.0)
         best[i] = top
         sums[i] = jnp.sum(shares, axis=-1, keepdims=True)
         acc[i] = jnp.dot(shares.astype(bf16), kv[me, i // RATIO, 1], preferred_element_type=f32)
 
-    def attend(i, slot):
-        scores = score_of(i, slot)
-        old = best[i]
-        top = jnp.maximum(old, jnp.max(scores, axis=-1, keepdims=True))
-        shares = jnp.exp(scores - top)
-        fading = jnp.exp(old - top)
-        best[i] = top
-        sums[i] = sums[i] * fading + jnp.sum(shares, axis=-1, keepdims=True)
-        acc[i] = acc[i] * fading + jnp.dot(
-            shares.astype(bf16), kv[slot, i // RATIO, 1], preferred_element_type=f32
-        )
+    def one_step(step, carry):
+        slot = me - step
+
+        def take(item):
+            hand_on(slot, item).wait_recv()
+
+            @pl.when(has_next)
+            def _():
+                hand_on(slot, item).start()
+
+        take(0)
+        take(gate_item)
+        for h in range(kv_here):
+            if h:
+                take(2 * h)
+            held = []
+            for i in range(h * RATIO, (h + 1) * RATIO):
+                scores = score_of(i, slot, gate_rows[slot, pl.ds(i, 1)])
+                old = best[i]
+                top = jnp.maximum(old, jnp.max(scores, axis=-1, keepdims=True))
+                shares = jnp.exp(scores - top)
+                fading = jnp.exp(old - top)
+                best[i] = top
+                sums[i] = sums[i] * fading + jnp.sum(shares, axis=-1, keepdims=True)
+                held.append((i, shares.astype(bf16), fading))
+            take(2 * h + 1)
+            for i, shares, fading in held:
+                acc[i] = acc[i] * fading + jnp.dot(
+                    shares, kv[slot, h, 1], preferred_element_type=f32
+                )
+        return carry
+
+    lax.fori_loop(1, jnp.minimum(me, 1) + 1, one_step, 0)
 
     @pl.when(has_prev)
     def _():
@@ -259,25 +284,7 @@
             mixing * pool_scale[:, cols]
         ).astype(bf16)
 
-    def one_step(step, carry):
-        slot = me - step
-
-        def take(item):
-            hand_on(slot, item).wait_recv()
-
-            @pl.when(has_next)
-            def _():
-                hand_on(slot, item).start()
-
-        take(gate_item)
-        for h in range(kv_here):
-            take(2 * h)
-            take(2 * h + 1)
-            for r in range(RATIO):
-                attend(h * RATIO + r, slot)
-        return carry
-
-    lax.fori_loop(1, me + 1, one_step, 0)
+    lax.fori_loop(2, me + 1, one_step, 0)
     for i in range(heads):
         act[:, i * HEAD : (i + 1) * HEAD] = (acc[i] / sums[i]).astype(bf16)
 
@@ -401,7 +408,8 @@
             pltpu.VMEM(q.shape, bf16),
             pltpu.VMEM(k.shape, bf16),
             pltpu.VMEM((n_sp, kv_here, 2, length, HEAD), bf16),
-            pltpu.VMEM((n_sp, 8, length), f32),
+            pltpu.VMEM((n_sp, heads, length), f32),
+            pltpu.VMEM((heads, length, 1), f32),
             pltpu.VMEM((heads, length, HEAD), bf16),
             pltpu.VMEM((heads, length, 1), f32),
             pltpu.VMEM((heads, length, 1), f32),
@@ -435,7 +443,7 @@
         k,
         v,
         p,
-        gates,
+        gates.T,
         q_gain.reshape(1, -1),
         k_gain.reshape(1, -1),
         pool_weight,

time: 59 us -> 56.3 us (0.954)
  local copies, waits for them, and re-layouts: 3.57 us -> 2.06 us
  Pallas kernels: 54.9 us -> 54.1 us
    unnamed x2 -> x1, local copies, waits for them, and re-layouts: 3.57 us -> 2.06 us
    pallas_call x1, Pallas kernels: 54.9 us -> 54.1 us  [body(): pl.pallas_call(functools.partial(kernel, n_sp, n_tp), out_shape=jax.Shape...]
where the time goes in v2:
time: 56.3 us; the launch traced here: 56.2 us
  Pallas kernels  54.1 us (96%)
  local copies, waits for them, and re-layouts  2.06 us (4%)
    pallas_call x1, Pallas kernels, body(): pl.pallas_call(functools.partial(kernel, n_sp, n_tp), out_shape=jax.Shape...  54.1 us
    unnamed x1, local copies, waits for them, and re-layouts  2.06 us

profile of v2, /device:TPU:28, one launch (start us, length us, event | category | flops | bytes accessed | tf_op | source)
XLA Modules:
  0.0 56.2 jit_solution(13962663232711801989)
XLA Ops:
  0.0 54.1 %mixer.1 = bf16[96,4096]{1,0:T(8,128)(2,1)} custom-call(bf16[384,512]{1,0:T(8,128)(2,1)} %q_hbm.1, bf16[384,256]{1,0:T(8,128)(2,1)} %k_hbm.1, bf16[384,256]{1,0:T(8,128)(2,1)} %v_hbm.1, bf16[384,512]{1,0:T(8,128)(2,1)} %p_hbm.1, f32[4,384]{1,0:T(4,128)} %bitcast.4, f32[1,128]{1,0:T(1,128)} %bitcast.6, f32[1,128]{1,0:T(1,128)} %bitcast.7, ...), custom_call_target="tpu_custom_call" | custom-call | tf_op jit(solution)/shard_map/mixer/pallas_call | solution.py:402
  54.1 2.1 %copy.13 = bf16[96,4096]{1,0:T(8,128)(2,1)} copy(bf16[96,4096]{1,0:T(8,128)(2,1)} %mixer.1) | data formatting | bytes 1572864

commit v3 on v2

--- a/solution.py
+++ b/solution.py
@@ -63,6 +63,8 @@
     x_in,
     own,
     out_buf,
+    relay_in,
+    relay_mid,
     in_sems,
     w_sems,
     kv_send,
@@ -72,6 +74,10 @@
     d_recv,
     x_send,
     x_recv,
+    relay_recv,
+    mid_send,
+    mid_recv,
+    back_send,
     out_sems,
 ):
     length = q_raw.shape[0]
@@ -84,6 +90,7 @@
     chip_rows = 2 * rows_out
     chunks = weights.shape[0]
     gate_item = 2 * kv_here
+    relayed = relay_in.shape[1]
 
     me = lax.axis_index("sp")
     tp = lax.axis_index("tp")
@@ -92,6 +99,9 @@
     partner = x * 2 + (1 - c)
     has_next = me < n_sp - 1
     has_prev = me > 0
+    relay_at = max(n_sp - 3, 0)
+    by_relay = jnp.logical_and(me == n_sp - 1, n_sp >= 3)
+    is_relay = jnp.logical_and(me == n_sp - 3, n_sp >= 3)
 
     def across(dx):
         return lax.rem(x + dx, n_x) * 2 + c
@@ -138,6 +148,14 @@
     def _():
         greet({"sp": me - 1})
 
+    @pl.when(by_relay)
+    def _():
+        greet({"sp": relay_at})
+
+    @pl.when(is_relay)
+    def _():
+        greet({"sp": n_sp - 1})
+
     greet({"tp": partner})
     for dx in range(1, n_x):
         greet({"tp": across(dx)})
@@ -151,7 +169,10 @@
         copy.wait()
     ins[1].wait()
 
-    pl.semaphore_wait(barrier, n_x + has_next.astype(jnp.int32) + has_prev.astype(jnp.int32))
+    peers = n_x
+    for linked in (has_next, has_prev, by_relay, is_relay):
+        peers = peers + linked.astype(jnp.int32)
+    pl.semaphore_wait(barrier, peers)
 
     after = jnp.minimum(me + 1, n_sp - 1)
 
@@ -311,6 +332,36 @@
             device_id_type=MESH,
         )
 
+    def to_relay(dx, r):
+        return pltpu.make_async_remote_copy(
+            src_ref=x_out.at[dx - 1, 2 * r + 1],
+            dst_ref=relay_in.at[dx - 1, r],
+            send_sem=x_send.at[dx - 1, 2 * r + 1],
+            recv_sem=relay_recv.at[dx - 1, r],
+            device_id={"sp": relay_at},
+            device_id_type=MESH,
+        )
+
+    def at_relay(dx, r):
+        return pltpu.make_async_remote_copy(
+            src_ref=relay_in.at[dx - 1, r],
+            dst_ref=relay_mid.at[dx - 1, r],
+            send_sem=mid_send.at[dx - 1, r],
+            recv_sem=mid_recv.at[dx - 1, r],
+            device_id={"tp": across(dx)},
+            device_id_type=MESH,
+        )
+
+    def from_relay(dx, r):
+        return pltpu.make_async_remote_copy(
+            src_ref=relay_mid.at[dx - 1, r],
+            dst_ref=x_in.at[dx - 1, 2 * r + 1],
+            send_sem=back_send.at[dx - 1, r],
+            recv_sem=x_recv.at[dx - 1, 2 * r + 1],
+            device_id={"sp": n_sp - 1},
+            device_id_type=MESH,
+        )
+
     def project(dx, j):
         top_row = pl.multiple_of(lax.rem(x + dx, n_x) * chip_rows, 16)
         part[dx, j] = jnp.dot(
@@ -331,7 +382,17 @@
                 own[j] = total
             else:
                 x_out[dx - 1, j] = total.astype(bf16)
-                x_copy(dx, j).start()
+                detour = jnp.logical_and(
+                    by_relay, jnp.logical_and(lax.rem(j, 2) == 1, j < 2 * relayed)
+                )
+
+                @pl.when(detour)
+                def _():
+                    to_relay(dx, j // 2).start()
+
+                @pl.when(jnp.logical_not(detour))
+                def _():
+                    x_copy(dx, j).start()
 
         def one_chunk(j, carry, dx=dx, finish=finish):
             project(dx, j)
@@ -343,7 +404,7 @@
             return carry
 
         lax.fori_loop(0, chunks, one_chunk, 0)
-        finish(chunks - 1)
+        finish(jnp.int32(chunks - 1))
 
     def out_copy(j):
         return pltpu.make_async_copy(
@@ -362,6 +423,22 @@
         return carry
 
     lax.fori_loop(0, chunks, last, 0)
+
+    @pl.when(is_relay)
+    def _():
+        lag = 2
+        for r in range(relayed + lag):
+            for dx in range(1, n_x):
+                if r < relayed:
+                    to_relay(dx, r).wait_recv()
+                    at_relay(dx, r).start()
+                if r >= lag:
+                    at_relay(dx, r - lag).wait_recv()
+                    from_relay(dx, r - lag).start()
+        for r in range(relayed):
+            for dx in range(1, n_x):
+                at_relay(dx, r).wait_send()
+                from_relay(dx, r).wait_send()
 
     def drain(j, carry):
         out_copy(j).wait()
@@ -423,6 +500,8 @@
             pltpu.VMEM((far, chunks, rows_out, CHUNK), bf16),
             pltpu.VMEM((chunks, rows_out, CHUNK), f32),
             pltpu.VMEM((chunks, rows_out, CHUNK), bf16),
+            pltpu.VMEM((far, max(chunks // 4, 1), rows_out, CHUNK), bf16),
+            pltpu.VMEM((far, max(chunks // 4, 1), rows_out, CHUNK), bf16),
             dma((3 + kv_here,)),
             dma((2 * chunks,)),
             dma((n_sp, items)),
@@ -432,6 +511,10 @@
             dma((n_x, chunks)),
             dma((far, chunks)),
             dma((far, chunks)),
+            dma((far, max(chunks // 4, 1))),
+            dma((far, max(chunks // 4, 1))),
+            dma((far, max(chunks // 4, 1))),
+            dma((far, max(chunks // 4, 1))),
             dma((chunks,)),
         ],
         compiler_params=pltpu.CompilerParams(

time: 56.3 us -> 56.5 us (level)
  no operation moved by 1% of the time
where the time goes in v3:
time: 56.5 us; the launch traced here: 56.4 us
  Pallas kernels  54.3 us (96%)
  local copies, waits for them, and re-layouts  2.06 us (4%)
    pallas_call x1, Pallas kernels, body(): pl.pallas_call(functools.partial(kernel, n_sp, n_tp), out_shape=jax.Shape...  54.3 us
    unnamed x1, local copies, waits for them, and re-layouts  2.06 us

profile of v3, /device:TPU:28, one launch (start us, length us, event | category | flops | bytes accessed | tf_op | source)
XLA Modules:
  0.0 56.4 jit_solution(10604534339685798934)
XLA Ops:
  0.0 54.3 %mixer.1 = bf16[96,4096]{1,0:T(8,128)(2,1)} custom-call(bf16[384,512]{1,0:T(8,128)(2,1)} %q_hbm.1, bf16[384,256]{1,0:T(8,128)(2,1)} %k_hbm.1, bf16[384,256]{1,0:T(8,128)(2,1)} %v_hbm.1, bf16[384,512]{1,0:T(8,128)(2,1)} %p_hbm.1, f32[4,384]{1,0:T(4,128)} %bitcast.4, f32[1,128]{1,0:T(1,128)} %bitcast.6, f32[1,128]{1,0:T(1,128)} %bitcast.7, ...), custom_call_target="tpu_custom_call" | custom-call | tf_op jit(solution)/shard_map/mixer/pallas_call | solution.py:479
  54.3 2.1 %copy.13 = bf16[96,4096]{1,0:T(8,128)(2,1)} copy(bf16[96,4096]{1,0:T(8,128)(2,1)} %mixer.1) | data formatting | bytes 1572864

commit v4 on v3

--- a/solution.py
+++ b/solution.py
@@ -87,7 +87,6 @@
     att_w = heads * HEAD
     n_x = n_tp // 2
     rows_out = length // n_tp
-    chip_rows = 2 * rows_out
     chunks = weights.shape[0]
     gate_item = 2 * kv_here
     relayed = relay_in.shape[1]
@@ -312,9 +311,13 @@
     for copy in loads:
         copy.wait()
 
+    def block_rows(dx, core):
+        first_row = (lax.rem(x + dx, n_x) * 2 + core) * rows_out
+        return pl.ds(pl.multiple_of(first_row, 16), rows_out)
+
     def pair_copy(dx, j):
         return pltpu.make_async_remote_copy(
-            src_ref=part.at[dx, j, pl.ds(pl.multiple_of((1 - c) * rows_out, 16), rows_out)],
+            src_ref=part.at[j, block_rows(dx, 1 - c)],
             dst_ref=pair_in.at[dx, j],
             send_sem=d_send.at[dx, j],
             recv_sem=d_recv.at[dx, j],
@@ -362,49 +365,44 @@
             device_id_type=MESH,
         )
 
-    def project(dx, j):
-        top_row = pl.multiple_of(lax.rem(x + dx, n_x) * chip_rows, 16)
-        part[dx, j] = jnp.dot(
-            act[pl.ds(top_row, chip_rows)], weights[j], preferred_element_type=f32
-        ).astype(bf16)
-        pair_copy(dx, j).start()
-
-    def pair_sum(dx, j):
-        pair_copy(dx, j).wait_recv()
-        mine = part[dx, j, pl.ds(pl.multiple_of(c * rows_out, 16), rows_out)]
-        return mine.astype(f32) + pair_in[dx, j].astype(f32)
-
-    for dx in list(range(1, n_x)) + [0]:
-
-        def finish(j, dx=dx):
-            total = pair_sum(dx, j)
+    order = list(range(1, n_x)) + [0]
+
+    def project(j):
+        part[j] = jnp.dot(act[...], weights[j], preferred_element_type=f32).astype(bf16)
+        for dx in order:
+            pair_copy(dx, j).start()
+
+    def finish(j):
+        for dx in order:
+            pair_copy(dx, j).wait_recv()
+            total = part[j, block_rows(dx, c)].astype(f32) + pair_in[dx, j].astype(f32)
             if dx == 0:
                 own[j] = total
-            else:
-                x_out[dx - 1, j] = total.astype(bf16)
-                detour = jnp.logical_and(
-                    by_relay, jnp.logical_and(lax.rem(j, 2) == 1, j < 2 * relayed)
-                )
-
-                @pl.when(detour)
-                def _():
-                    to_relay(dx, j // 2).start()
-
-                @pl.when(jnp.logical_not(detour))
-                def _():
-                    x_copy(dx, j).start()
-
-        def one_chunk(j, carry, dx=dx, finish=finish):
-            project(dx, j)
-
-            @pl.when(j > 0)
+                continue
+            x_out[dx - 1, j] = total.astype(bf16)
+            detour = jnp.logical_and(
+                by_relay, jnp.logical_and(lax.rem(j, 2) == 1, j < 2 * relayed)
+            )
+
+            @pl.when(detour)
             def _():
-                finish(j - 1)
-
-            return carry
-
-        lax.fori_loop(0, chunks, one_chunk, 0)
-        finish(jnp.int32(chunks - 1))
+                to_relay(dx, j // 2).start()
+
+            @pl.when(jnp.logical_not(detour))
+            def _():
+                x_copy(dx, j).start()
+
+    def one_chunk(j, carry):
+        project(j)
+
+        @pl.when(j > 0)
+        def _():
+            finish(j - 1)
+
+        return carry
+
+    lax.fori_loop(0, chunks, one_chunk, 0)
+    finish(jnp.int32(chunks - 1))
 
     def out_copy(j):
         return pltpu.make_async_copy(
@@ -494,7 +492,7 @@
             pltpu.VMEM((length + RIM, p.shape[1]), bf16),
             pltpu.VMEM((length, depth), bf16),
             pltpu.VMEM((chunks, depth, CHUNK), bf16),
-            pltpu.VMEM((n_x, chunks, 2 * rows_out, CHUNK), bf16),
+            pltpu.VMEM((chunks, length, CHUNK), bf16),
             pltpu.VMEM((n_x, chunks, rows_out, CHUNK), bf16),
             pltpu.VMEM((far, chunks, rows_out, CHUNK), bf16),
             pltpu.VMEM((far, chunks, rows_out, CHUNK), bf16),

time: 56.5 us -> 53.6 us (0.949)
  Pallas kernels: 54.3 us -> 51.1 us
    pallas_call x1, Pallas kernels: 54.3 us -> 51.1 us  [body(): pl.pallas_call(functools.partial(kernel, n_sp, n_tp), out_shape=jax.Shape...]
where the time goes in v4:
time: 53.6 us; the launch traced here: 53.2 us
  Pallas kernels  51.1 us (95%)
  local copies, waits for them, and re-layouts  2.06 us (4%)
    pallas_call x1, Pallas kernels, body(): pl.pallas_call(functools.partial(kernel, n_sp, n_tp), out_shape=jax.Shape...  51.1 us
    unnamed x1, local copies, waits for them, and re-layouts  2.06 us

profile of v4, /device:TPU:28, one launch (start us, length us, event | category | flops | bytes accessed | tf_op | source)
XLA Modules:
  0.0 53.2 jit_solution(362278164445525427)
XLA Ops:
  0.0 51.1 %mixer.1 = bf16[96,4096]{1,0:T(8,128)(2,1)} custom-call(bf16[384,512]{1,0:T(8,128)(2,1)} %q_hbm.1, bf16[384,256]{1,0:T(8,128)(2,1)} %k_hbm.1, bf16[384,256]{1,0:T(8,128)(2,1)} %v_hbm.1, bf16[384,512]{1,0:T(8,128)(2,1)} %p_hbm.1, f32[4,384]{1,0:T(4,128)} %bitcast.4, f32[1,128]{1,0:T(1,128)} %bitcast.6, f32[1,128]{1,0:T(1,128)} %bitcast.7, ...), custom_call_target="tpu_custom_call" | custom-call | tf_op jit(solution)/shard_map/mixer/pallas_call | solution.py:477
  51.1 2.1 %copy.13 = bf16[96,4096]{1,0:T(8,128)(2,1)} copy(bf16[96,4096]{1,0:T(8,128)(2,1)} %mixer.1) | data formatting | bytes 1572864
